TPU v7x, 32 devices: a whole 2x2x4 slice. The times are simulated.
32 devices in a mesh: sp: 8 (over z, y), tp: 4 (over x, core).
Axes of the slice: x: 2, y: 2, z: 4, core: 2. Of those that a mesh axis runs over, the one named last changes fastest.
Arguments:
- tokens: bfloat16 [2048, 4096], P('sp'), may hold values from -6 to 6
- norm_gain: float32 [4096], replicated, may hold values from 0.1 to 1.9
- w_query: bfloat16 [4096, 512], P('sp', 'tp'), may hold values from -0.09375 to 0.09375
- w_key: bfloat16 [4096, 512], P('sp', 'tp'), may hold values from -0.09375 to 0.09375
- w_value: bfloat16 [4096, 1024], P('sp', 'tp'), may hold values from -0.09375 to 0.09375
- w_gates: bfloat16 [4096, 2, 2, 4], P(None, None, None, 'tp'), may hold values from -0.09375 to 0.09375
- input_bias: float32 [2, 4], P(None, 'tp'), may hold values from -2 to 90
- forget_bias: float32 [2, 4], P(None, 'tp'), as said below
- decay_shift: float32 [2, 2048, 4], P(None, 'sp', 'tp'), may hold values from -2.5 to 0
- head_gain: float32 [1024], P('tp'), may hold values from 0.1 to 1.9
- w_conv_b: bfloat16 [4096, 1024], P('sp', 'tp'), may hold values from -0.09375 to 0.09375
- w_conv_c: bfloat16 [4096, 1024], P('sp', 'tp'), may hold values from -0.09375 to 0.09375
- w_conv_in: bfloat16 [4096, 1024], P('sp', 'tp'), may hold values from -0.09375 to 0.09375
- conv_taps: bfloat16 [3, 1024], P(None, 'tp'), may hold values from -3.5 to 3.5
- w_out: bfloat16 [2048, 4096], P('sp', 'tp'), may hold values from -0.125 to 0.125
Outputs:
- mixed_out: bfloat16 [2048, 4096], P('sp', 'tp')
Inputs may be any that keep to these rules, and one draw needn't show every extreme that they name: `forget_bias`: at most the natural logarithm of 2048 plus 2.
All inputs are finite; a program needn't handle non-finite values.
Results may differ from a plain program's by a relative error of at most 0.02.
Values may be sent and summed in bfloat16 or wider, within the bound.
A program may use at most 128 MiB of HBM per device.

v0:
```python
import jax
import jax.numpy as jnp
from jax import lax
from jax.sharding import PartitionSpec as P

DQK = 128
DV = 256
BLOCK = 128
EPS = 1e-06
HIGH = lax.Precision.HIGHEST
LOWEST = -1e30


def carried_in(value, axis, join, neutral, backward):
    count, mine = (lax.axis_size(axis), lax.axis_index(axis))
    pieces = jax.tree.map(lambda part: lax.all_gather(part, axis), value)
    if backward:
        pieces = jax.tree.map(lambda part: part[::-1], pieces)
        mine = count - 1 - mine
    subtotal = jax.tree.map(
        lambda part, zero: jnp.full_like(part, 0) + jnp.asarray(zero, part.dtype), value, neutral
    )

    def lap(position, subtotal):
        longer = join(subtotal, jax.tree.map(lambda part: part[position], pieces))
        return jax.tree.map(lambda new, old: jnp.where(position < mine, new, old), longer, subtotal)

    return lax.fori_loop(0, count - 1, lap, subtotal)


def padded_2(value, sides, width):
    for axis, dim in sides:
        size, length = (lax.axis_size(axis), value.shape[dim])
        up = [(i, (i + 1) % size) for i in range(size - 1)]
        down = [(j, i) for i, j in up]
        last = lax.slice_in_dim(value, length - width, length, axis=dim)
        initial = lax.slice_in_dim(value, 0, width, axis=dim)
        before = lax.ppermute(last, axis, up)
        after = lax.ppermute(initial, axis, down)
        value = jnp.concatenate([before, value, after], axis=dim)
    return value


def row_norm(tokens, norm_gain):
    values = tokens.astype(jnp.float32)
    inverse_rms = lax.rsqrt(jnp.mean(values * values, axis=-1, keepdims=True) + EPS)
    return (values * inverse_rms * norm_gain).astype(jnp.bfloat16)


def to_heads(source, head_count):
    length = source.shape[0]
    return source.astype(jnp.float32).reshape(length, head_count, -1).transpose(1, 0, 2)


def combine(earlier, later):
    total_a, memory_a, normer_a, stable_a = earlier
    total_b, memory_b, normer_b, stable_b = later
    stable = jnp.maximum(stable_a + total_b, stable_b)
    weight_a = jnp.exp(stable_a + total_b - stable)
    weight_b = jnp.exp(stable_b - stable)
    memory = weight_a[..., None, None] * memory_a + weight_b[..., None, None] * memory_b
    normer = weight_a[..., None] * normer_a + weight_b[..., None] * normer_b
    return (total_a + total_b, memory, normer, stable)


def local_pass(queries, keys_all, values_all, in_gate, log_forget, backward):
    head_count, length = in_gate.shape
    block_count = length // BLOCK

    def blocked(source):
        return source.reshape((head_count, block_count, BLOCK) + source.shape[2:])

    query_block = blocked(queries)
    key_blk = blocked(keys_all)
    value_blk = blocked(values_all)
    gate_blk = blocked(in_gate)
    cumulative = jnp.cumsum(blocked(log_forget), axis=-1)
    block_total = cumulative[..., -1]
    log_update = block_total[..., None] - cumulative + gate_blk
    block_stable = jnp.max(log_update, axis=-1)
    update = jnp.exp(log_update - block_stable[..., None])
    block_memory = jnp.einsum(
        "hcsv,hcsd->hcvd", value_blk * update[..., None], key_blk, precision=HIGH
    )
    block_normer = jnp.einsum("hcs,hcsd->hcd", update, key_blk, precision=HIGH)
    identity = (
        jnp.zeros((head_count,), jnp.float32),
        jnp.zeros((head_count, DV, DQK), jnp.float32),
        jnp.zeros((head_count, DQK), jnp.float32),
        jnp.full((head_count,), LOWEST, jnp.float32),
    )
    running = identity
    prefixes = []
    for index in range(block_count):
        prefixes.append(running)
        running = combine(
            running,
            (
                block_total[:, index],
                block_memory[:, index],
                block_normer[:, index],
                block_stable[:, index],
            ),
        )
    if backward:
        incoming = carried_in(running, "sp", combine, identity, True)
    else:
        incoming = carried_in(running, "sp", combine, identity, False)
    stacked = tuple((jnp.stack(members, axis=1) for members in zip(*prefixes)))
    expanded = tuple((member[:, None] for member in incoming))
    ignored, start_memory, start_normer, start_stable = combine(expanded, stacked)
    lower_mask = jnp.tril(jnp.ones((BLOCK, BLOCK), dtype=bool))
    log_weight = jnp.where(
        lower_mask,
        cumulative[..., :, None] - cumulative[..., None, :] + gate_blk[..., None, :],
        -jnp.inf,
    )
    carried = cumulative + start_stable[..., None]
    running_max = jnp.maximum(carried, jnp.max(log_weight, axis=-1))
    scores = jnp.einsum("hctd,hcsd->hcts", query_block, key_blk, precision=HIGH) * jnp.exp(
        log_weight - running_max[..., None]
    )
    carry_weight = jnp.exp(carried - running_max)
    numerator = jnp.einsum("hcts,hcsv->hctv", scores, value_blk, precision=HIGH) + carry_weight[
        ..., None
    ] * jnp.einsum("hcvd,hctd->hctv", start_memory, query_block, precision=HIGH)
    denominator = jnp.sum(scores, axis=-1) + carry_weight * jnp.einsum(
        "hcd,hctd->hct", start_normer, query_block, precision=HIGH
    )
    result = numerator / jnp.maximum(jnp.abs(denominator), jnp.exp(-running_max))[..., None]
    return result.reshape(head_count, length, DV)


def flipped(source):
    return jnp.flip(source, axis=1)


def lstm_branch(
    normed,
    query_proj,
    key_proj,
    value_proj,
    w_gates,
    input_bias,
    forget_bias,
    decay_shift,
    head_gain,
):
    length = normed.shape[0]
    head_count = w_gates.shape[-1]
    gate_pre = jnp.dot(
        normed,
        w_gates.reshape(w_gates.shape[0], 4 * head_count),
        preferred_element_type=jnp.float32,
    ).reshape(length, 2, 2, head_count)
    queries = to_heads(query_proj, head_count) * DQK ** (-0.5)
    keys_all = to_heads(key_proj, head_count)
    values_all = to_heads(value_proj, head_count)
    summed = jnp.zeros((head_count, length, DV), jnp.float32)
    for direction in range(2):
        in_gate = (gate_pre[:, direction, 0, :] + input_bias[direction]).T
        log_forget = (
            jax.nn.log_sigmoid(gate_pre[:, direction, 1, :] + forget_bias[direction])
            + decay_shift[direction]
        ).T
        if direction == 1:
            result = flipped(
                local_pass(
                    flipped(queries),
                    flipped(keys_all),
                    flipped(values_all),
                    flipped(in_gate),
                    flipped(log_forget),
                    True,
                )
            )
        else:
            result = local_pass(queries, keys_all, values_all, in_gate, log_forget, False)
        summed = summed + result
    inverse_rms = lax.rsqrt(jnp.mean(summed * summed, axis=-1, keepdims=True) + EPS)
    return ((summed * inverse_rms).transpose(1, 0, 2) * head_gain.reshape(head_count, DV)).astype(
        jnp.bfloat16
    )


def conv_branch(gate_outer, gate_inner, conv_input, conv_taps):
    length = gate_outer.shape[0]
    mixed_in = (gate_inner.astype(jnp.float32) * conv_input.astype(jnp.float32)).astype(
        jnp.bfloat16
    )
    padded = padded_2(mixed_in, (("sp", 0),), 1).astype(jnp.float32)
    taps_wide = conv_taps.astype(jnp.float32)
    filtered = taps_wide[0] * padded[:-2] + taps_wide[1] * padded[1:-1] + taps_wide[2] * padded[2:]
    return (gate_outer.astype(jnp.float32) * filtered).astype(jnp.bfloat16).reshape(length, -1, DV)


def projected(normed, matrices):
    return tuple(
        (
            jnp.dot(normed, matrix, preferred_element_type=jnp.float32).astype(jnp.bfloat16)
            for matrix in matrices
        )
    )


def body(
    tokens,
    norm_gain,
    w_query,
    w_key,
    w_value,
    w_gates,
    input_bias,
    forget_bias,
    decay_shift,
    head_gain,
    w_conv_b,
    w_conv_c,
    w_conv_in,
    conv_taps,
    w_out,
):
    normed = row_norm(tokens, norm_gain)
    length = normed.shape[0]
    whole_mats = (
        lax.all_gather(w_query, "sp", axis=0, tiled=True),
        lax.all_gather(w_key, "sp", axis=0, tiled=True),
        lax.all_gather(w_value, "sp", axis=0, tiled=True),
        lax.all_gather(w_conv_b, "sp", axis=0, tiled=True),
        lax.all_gather(w_conv_c, "sp", axis=0, tiled=True),
        lax.all_gather(w_conv_in, "sp", axis=0, tiled=True),
    )
    query_proj, key_proj, value_proj, gate_outer, gate_inner, conv_input = projected(
        normed, whole_mats
    )
    lstm_out = lstm_branch(
        normed,
        query_proj,
        key_proj,
        value_proj,
        w_gates,
        input_bias,
        forget_bias,
        decay_shift,
        head_gain,
    )
    conv_out = conv_branch(gate_outer, gate_inner, conv_input, conv_taps)
    joined = jnp.stack([lstm_out, conv_out], axis=2).reshape(length, -1)
    joined_all = lax.all_gather(joined, "tp", axis=1, tiled=True)
    out_whole = lax.all_gather(w_out, "sp", axis=0, tiled=True)
    return jnp.dot(joined_all, out_whole, preferred_element_type=jnp.float32).astype(jnp.bfloat16)


def solution(mesh):
    placed = (
        P("sp", None),
        P(),
        P("sp", "tp"),
        P("sp", "tp"),
        P("sp", "tp"),
        P(None, None, None, "tp"),
        P(None, "tp"),
        P(None, "tp"),
        P(None, "sp", "tp"),
        P("tp"),
        P("sp", "tp"),
        P("sp", "tp"),
        P("sp", "tp"),
        P(None, "tp"),
        P("sp", "tp"),
    )
    return jax.shard_map(body, mesh=mesh, in_specs=placed, out_specs=P("sp", "tp"), check_vma=False)
```

profile of v0, /device:TPU:0, one launch (start us, length us, event | category | flops | bytes accessed | tf_op | source)
XLA Modules:
  0.0 511.0 jit_solution(5849541648931565221)
XLA Ops:
  23.6 3.6 fusion.84
  32.9 3.7 fusion.87
  37.9 23.7 %all-reduce.8 = (f32[8]{0:T(128)}, f32[8]{0:T(128)}, f32[8]{0:T(128)S(1)}, f32[8]{0:T(128)S(1)}) all-reduce(f32[8]{0:T(128)S(1)} %fusion.66, f32[8]{0:T(128)S(1)} %dynamic-update-slice.1, f32[8]{0:T(128)S(1)} %fusion.65, f32[8]{0:T(128)S(1)} %dynamic-update-slice.3), channel_id=2, replica_groups=mesh['sp'=8,'tp'=4] {'sp'}, use_global_device_ids=true, to_apply=%add.4 | all-reduce | flops 32 | bytes 256
  78.7 15.1 %all-gather.15.cloned.1.call-done = bf16[4096,128]{1,0:T(8,128)(2,1)} async-done(((bf16[512,128]{1,0:T(8,128)(2,1)}), bf16[4096,128]{1,0:T(8,128)(2,1)}) %all-gather.15.cloned.1.call-update) | async-done | bytes 1048592 | tf_op jit(solution)/shard_map/all_gather | solution.py:226
  93.8 2.6 broadcast_multiply_fusion.1
  96.4 47.4 %all-gather.19.cloned.1.call-done = bf16[4096,256]{1,0:T(8,128)(2,1)} async-done(((bf16[512,256]{1,0:T(8,128)(2,1)}), bf16[4096,256]{1,0:T(8,128)(2,1)}) %all-gather.19.cloned.1.call-update) | async-done | bytes 2097168 | tf_op jit(solution)/shard_map/all_gather | solution.py:228
  143.8 2.3 fusion.83
  147.8 18.2 %all_gather.78 = f32[8,1,128]{2,1,0:T(1,128)S(1)} all-gather(f32[1,1,128]{2,1,0:T(1,128)S(1)} %get-tuple-element.431), channel_id=1, replica_groups=mesh['sp'=8,'tp'=4] {'sp'}, dimensions={0}, use_global_device_ids=true | all-gather | bytes 4608 | tf_op jit(solution)/shard_map/all_gather | solution.py:16
  167.1 17.2 %all_gather.72 = f32[8,1,128]{2,1,0:T(1,128)} all-gather(f32[1,1,128]{2,1,0:T(1,128)S(1)} %get-tuple-element.439), channel_id=1, replica_groups=mesh['sp'=8,'tp'=4] {'sp'}, dimensions={0}, use_global_device_ids=true | all-gather | bytes 4608 | tf_op jit(solution)/shard_map/all_gather | solution.py:16
  184.5 9.1 %all-gather.27.cloned.1.call-done = bf16[4096,256]{1,0:T(8,128)(2,1)} async-done(((bf16[512,256]{1,0:T(8,128)(2,1)}), bf16[4096,256]{1,0:T(8,128)(2,1)}) %all-gather.27.cloned.1.call-update) | async-done | bytes 2097168 | tf_op jit(solution)/shard_map/all_gather | solution.py:230
  193.7 2.5 fusion.20
  196.2 47.1 %all-gather.29.cloned.1.call-done = bf16[4096,256]{1,0:T(8,128)(2,1)} async-done(((bf16[512,256]{1,0:T(8,128)(2,1)}), bf16[4096,256]{1,0:T(8,128)(2,1)}) %all-gather.29.cloned.1.call-update) | async-done | bytes 2097168 | tf_op jit(solution)/shard_map/all_gather | solution.py:231
  243.3 2.5 fusion.19
  245.9 2.5 collective-permute-start
  252.0 3.9 collective-permute-done.1
  256.9 36.2 %all-gather.25.cloned.1.call-done = bf16[4096,256]{1,0:T(8,128)(2,1)} async-done(((bf16[512,256]{1,0:T(8,128)(2,1)}), bf16[4096,256]{1,0:T(8,128)(2,1)}) %all-gather.25.cloned.1.call-update) | async-done | bytes 2097168 | tf_op jit(solution)/shard_map/all_gather | solution.py:229
  293.1 3.3 fusion.24
  296.3 37.7 %all-gather.21.cloned.1.call-done = f32[8,1,256,128]{3,2,1,0:T(8,128)} async-done(((f32[1,1,256,128]{3,2,1,0:T(8,128)}), f32[8,1,256,128]{3,2,1,0:T(8,128)}) %all-gather.21.cloned.1.call-update) | async-done | bytes 1048592 | tf_op jit(solution)/shard_map/all_gather | solution.py:16
  334.1 29.4 %while.36 = (s32[]{:T(128)}, f32[1,256,128]{2,1,0:T(8,128)S(1)}, f32[1,128]{1,0:T(1,128)S(1)}, f32[1]{0:T(128)}, s32[]{:T(128)}, /*index=5*/f32[8,1]{0,1:T(1,128...) while((s32[]{:T(128)}, f32[1,256,128]{2,1,0:T(8,128)S(1)}, ...), condition=%wide.region_4.5_spmd.clone, body=%wide.region_3.4_spmd.clone.sunk | while | flops 164489 | bytes 395004 | solution.py:28
  363.5 11.7 %all-gather.23.cloned.1.call-done = f32[8,1,256,128]{3,2,1,0:T(8,128)} async-done(((f32[1,1,256,128]{3,2,1,0:T(8,128)}), f32[8,1,256,128]{3,2,1,0:T(8,128)}) %all-gather.23.cloned.1.call-update) | async-done | bytes 1048592 | tf_op jit(solution)/shard_map/all_gather | solution.py:16
  376.6 23.4 %while.37 = (s32[]{:T(128)}, f32[1,256,128]{2,1,0:T(8,128)S(1)}, f32[1,128]{1,0:T(1,128)S(1)}, f32[1]{0:T(128)}, s32[]{:T(128)}, /*index=5*/f32[8,1]{0,1:T(1,128...) while((s32[]{:T(128)}, f32[1,256,128]{2,1,0:T(8,128)S(1)}, ...), condition=%wide.region_10.11_spmd.clone, body=%wide.region_9.10_spmd.clone.sunk | while | flops 164489 | bytes 395004 | solution.py:28
  409.9 15.0 %all-gather.31.cloned.1.call-done = bf16[256,2048]{0,1:T(8,128)(2,1)} async-done(((bf16[256,512]{0,1:T(8,128)(2,1)}), bf16[256,2048]{0,1:T(8,128)(2,1)}) %all-gather.31.cloned.1.call-update) | async-done | bytes 1048592 | tf_op jit(solution)/shard_map/all_gather | solution.py:249
  424.8 74.8 %all-gather.33.cloned.1.call-done = bf16[2048,1024]{1,0:T(8,128)(2,1)} async-done(((bf16[256,1024]{1,0:T(8,128)(2,1)}), bf16[2048,1024]{1,0:T(8,128)(2,1)}) %all-gather.33.cloned.1.call-update) | async-done | bytes 4194320 | tf_op jit(solution)/shard_map/all_gather | solution.py:250
  499.6 4.6 convolution_convert_fusion
  (221 shorter events, 76.8 us)
Async XLA Ops:
  6.5 69.7 %all-gather.17.cloned.1.call-start = ((), (), s32[]{:S(2)}) async-start(), calls=%async_computation.1 | async-start | bytes 1179648 | tf_op jit(solution)/shard_map/all_gather | solution.py:227
  7.3 86.5 %all-gather.15.cloned.1.call-start = ((), (), s32[]{:S(2)}) async-start(), calls=%async_computation | async-start | bytes 1179648 | tf_op jit(solution)/shard_map/all_gather | solution.py:226
  8.0 135.7 %all-gather.19.cloned.1.call-start = ((), (), s32[]{:S(2)}) async-start(), calls=%async_computation.2 | async-start | bytes 2359296 | tf_op jit(solution)/shard_map/all_gather | solution.py:228
  8.8 184.9 %all-gather.27.cloned.1.call-start = ((), (), s32[]{:S(2)}) async-start(), calls=%async_computation.6 | async-start | bytes 2359296 | tf_op jit(solution)/shard_map/all_gather | solution.py:230
  9.3 233.9 %all-gather.29.cloned.1.call-start = ((), (), s32[]{:S(2)}) async-start(), calls=%async_computation.7 | async-start | bytes 2359296 | tf_op jit(solution)/shard_map/all_gather | solution.py:231
  9.9 283.2 %all-gather.25.cloned.1.call-start = ((), (), s32[]{:S(2)}) async-start(), calls=%async_computation.5 | async-start | bytes 2359296 | tf_op jit(solution)/shard_map/all_gather | solution.py:229
  10.5 323.5 %all-gather.21.cloned.1.call-start = ((), (), s32[]{:S(2)}) async-start(), calls=%async_computation.3 | async-start | bytes 1179648 | tf_op jit(solution)/shard_map/all_gather | solution.py:16
  16.2 59.4 %copy-start.23 = (bf16[3,256]{1,0:T(4,128)(2,1)S(1)}, bf16[3,256]{1,0:T(4,128)(2,1)}, u32[]{:S(2)}) copy-start(bf16[3,256]{1,0:T(4,128)(2,1)} %param.32) | copy-start | bytes 4612
  18.2 58.0 %copy-start.17 = (f32[256,1,1,1]{0,2,1,3:T(1,128)}, f32[256,1,1,1]{0,2,1,3:T(1,128)S(1)}, u32[]{:S(2)}) copy-start(f32[256,1,1,1]{0,2,1,3:T(1,128)S(1)} %get-tuple-element.451) | copy-start | bytes 3076
  18.6 57.7 %copy-start.9 = (f32[1,2,128]{2,1,0:T(2,128)}, f32[1,2,128]{2,1,0:T(2,128)S(1)}, u32[]{:S(2)}) copy-start(f32[1,2,128]{2,1,0:T(2,128)S(1)} %reduce_window_sum.17) | copy-start | bytes 3076
  28.8 47.5 %copy-start.6 = (f32[1,2,128]{2,1,0:T(2,128)}, f32[1,2,128]{2,1,0:T(2,128)S(1)}, u32[]{:S(2)}) copy-start(f32[1,2,128]{2,1,0:T(2,128)S(1)} %reduce_window_sum.18) | copy-start | bytes 3076
  32.0 44.2 %copy-start.12 = (f32[1,256]{1,0:T(1,128)}, f32[1,256]{1,0:T(1,128)S(1)}, u32[]{:S(2)}) copy-start(f32[1,256]{1,0:T(1,128)S(1)} %broadcast_add_fusion) | copy-start | bytes 3076
  78.2 68.0 %copy-start = (bf16[256,128]{1,0:T(8,128)(2,1)}, bf16[256,128]{1,0:T(8,128)(2,1)S(1)}, u32[]{:S(2)}) copy-start(bf16[256,128]{1,0:T(8,128)(2,1)S(1)} %convolution_convert_fusion.5) | copy-start | bytes 196612
  147.2 228.0 %all-gather.23.cloned.1.call-start = ((), (), s32[]{:S(2)}) async-start(), calls=%async_computation.4 | async-start | bytes 1179648 | tf_op jit(solution)/shard_map/all_gather | solution.py:16
  245.9 5.4 %collective-permute-start = (bf16[1,256]{0,1:T(8,128)(2,1)S(1)}, bf16[1,256]{0,1:T(8,128)(2,1)S(1)}, u32[]{:S(2)}, u32[]{:S(2)}) collective-permute-start(bf16[1,256]{0,1:T(8,128)(2,1)S(1)} %get-tuple-element.447), channel_id=1, source_target_pairs={{0,4},{4,8},{8,12},{12,16},{16,20},{20,24},{24,28},{1,5},{5,9},{9,... | collective-permute-start | bytes 1544 | tf_op jit(solution)/shard_map/ppermute | solution.py:38
  248.4 7.5 %collective-permute-start.1 = (bf16[1,256]{0,1:T(8,128)(2,1)S(1)}, bf16[1,256]{0,1:T(8,128)(2,1)}, u32[]{:S(2)}, u32[]{:S(2)}) collective-permute-start(bf16[1,256]{0,1:T(8,128)(2,1)S(1)} %get-tuple-element.448), channel_id=1, source_target_pairs={{4,0},{8,4},{12,8},{16,12},{20,16},{24,20},{28,24},{5,1},{9,5},{13... | collective-permute-start | bytes 1544 | tf_op jit(solution)/shard_map/ppermute | solution.py:39
  251.1 173.7 %all-gather.31.cloned.1.call-start = ((), (), s32[]{:S(2)}) async-start(), calls=%async_computation.8 | async-start | bytes 1310720 | tf_op jit(solution)/shard_map/all_gather | solution.py:249
  334.1 42.5 %copy-start.14 = (f32[1,128]{1,0:T(1,128)S(1)}, f32[1,128]{1,0:T(1,128)}, u32[]{:S(2)}) copy-start(f32[1,128]{1,0:T(1,128)} %custom-call.3) | copy-start | bytes 1540
  334.1 42.5 %copy-start.19 = (f32[8]{0:T(128)S(1)}, f32[8]{0:T(128)}, u32[]{:S(2)}) copy-start(f32[8]{0:T(128)} %reverse.17) | copy-start | bytes 100
  334.1 42.5 %copy-start.20 = (f32[8]{0:T(128)S(1)}, f32[8]{0:T(128)}, u32[]{:S(2)}) copy-start(f32[8]{0:T(128)} %reverse.18) | copy-start | bytes 100
  363.5 41.0 %copy-start.24 = (f32[2,128]{1,0:T(2,128)S(1)}, f32[2,128]{1,0:T(2,128)}, u32[]{:S(2)}) copy-start(f32[2,128]{1,0:T(2,128)} %get-tuple-element.383) | copy-start | bytes 3076
  363.5 41.0 %copy-start.25 = (f32[2,128]{1,0:T(2,128)S(1)}, f32[2,128]{1,0:T(2,128)}, u32[]{:S(2)}) copy-start(f32[2,128]{1,0:T(2,128)} %get-tuple-element.384) | copy-start | bytes 3076
  363.5 41.1 %copy-start.13 = (f32[1,256]{1,0:T(1,128)S(1)}, f32[1,256]{1,0:T(1,128)}, u32[]{:S(2)}) copy-start(f32[1,256]{1,0:T(1,128)} %copy-done.12) | copy-start | bytes 3076
  409.3 90.4 %all-gather.33.cloned.1.call-start = ((), (), s32[]{:S(2)}) async-start(), calls=%async_computation.9 | async-start | bytes 4718592 | tf_op jit(solution)/shard_map/all_gather | solution.py:250
  (22 other events, 344.0 us)
Sparse Core Ops, SparseCore 0:
  9.5 43.1 all-gather.16
  54.8 38.9 all-gather.14
  95.9 47.7 all-gather.18
  145.7 47.8 all-gather.26
  195.6 47.5 all-gather.28
  245.2 47.7 all-gather.24
  295.2 38.7 all-gather.20
  336.2 39.0 all-gather.22
  409.4 15.3 all-gather.30
  426.8 72.7 all-gather.32
where the time goes:
time: 513 us; the launch traced here: 511 us
  waiting for transfers between devices  302 us (59%)
  blocking collectives  59.1 us (12%)
  other arithmetic  48.9 us (10%)
  loops' own time  27.5 us (5%)
  matrix products  24.6 us (5%)
  local copies, waits for them, and re-layouts  22.3 us (4%)
  between operations  22.1 us (4%)
    all_gather x1, waiting for transfers between devices, body(): out_whole = lax.all_gather(w_out, 'sp', axis=0, tiled=True)  74.8 us
    all_gather x2, waiting for transfers between devices, carried_in(): pieces = jax.tree.map(lambda part: lax.all_gather(part, axis), value)  49.4 us
    all_gather x1, waiting for transfers between devices, body(): lax.all_gather(w_value, 'sp', axis=0, tiled=True)  47.4 us
    all_gather x1, waiting for transfers between devices, body(): lax.all_gather(w_conv_in, 'sp', axis=0, tiled=True)  47.1 us
    all_gather x1, waiting for transfers between devices, body(): lax.all_gather(w_conv_b, 'sp', axis=0, tiled=True)  36.2 us
    all_gather x2, blocking collectives, carried_in(): pieces = jax.tree.map(lambda part: lax.all_gather(part, axis), value)  35.4 us
    another operation x2, loops' own time, carried_in(): return lax.fori_loop(0, count - 1, lap, subtotal)  27.5 us
    unnamed x1, blocking collectives  23.7 us
  transfers between devices with their start and end apart: 12, of which 10 were waited for; matrix products, arithmetic and copies ran while one was open for 14% of the time, Pallas kernels for 0%

commit v1 on v0

--- a/solution.py
+++ b/solution.py
@@ -247,7 +247,12 @@
     conv_out = conv_branch(gate_outer, gate_inner, conv_input, conv_taps)
     joined = jnp.stack([lstm_out, conv_out], axis=2).reshape(length, -1)
     joined_all = lax.all_gather(joined, "tp", axis=1, tiled=True)
-    out_whole = lax.all_gather(w_out, "sp", axis=0, tiled=True)
+    ring = [w_out]
+    for hop in range(7):
+        ring.append(lax.ppermute(ring[-1], "sp", [(dev, (dev + 1) % 8) for dev in range(8)]))
+    out_whole = jnp.roll(
+        jnp.concatenate(ring[::-1], axis=0), (lax.axis_index("sp") + 1) * ring[0].shape[0], axis=0
+    )
     return jnp.dot(joined_all, out_whole, preferred_element_type=jnp.float32).astype(jnp.bfloat16)
 
 

time: 513 us -> 482 us (0.940)
  waiting for transfers between devices: 302 us -> 215 us
  local copies, waits for them, and re-layouts: 22.3 us -> 56.1 us
  starting transfers between devices: 4.32 us -> 12.1 us
  other arithmetic: 48.9 us -> 55.9 us
    all_gather x1 -> x0, waiting for transfers between devices: 74.8 us -> none  [body(): out_whole = lax.all_gather(w_out, 'sp', axis=0, tiled=True)]
    ppermute x0 -> x7, waiting for transfers between devices: none -> 50.7 us  [body(): lax.ppermute(ring[-1], 'sp', [(dev, (dev + 1) % 8) for dev in range(8)])]
    unnamed x75 -> x78, local copies, waits for them, and re-layouts: 5.29 us -> 29.7 us
    all_gather x1, waiting for transfers between devices: 47.4 us -> 29.2 us  [body(): lax.all_gather(w_value, 'sp', axis=0, tiled=True)]
    all_gather x1, waiting for transfers between devices: 15.1 us -> 0.01 us  [body(): lax.all_gather(w_query, 'sp', axis=0, tiled=True)]
    all_gather x1, waiting for transfers between devices: 15 us -> 0.01 us  [body(): joined_all = lax.all_gather(joined, 'tp', axis=1, tiled=True)]
    all_gather x2, waiting for transfers between devices: 49.4 us -> 40.2 us  [carried_in(): pieces = jax.tree.map(lambda part: lax.all_gather(part, axis), value)]
    ppermute x0 -> x7, starting transfers between devices: none -> 7.28 us  [body(): lax.ppermute(ring[-1], 'sp', [(dev, (dev + 1) % 8) for dev in range(8)])]
  transfers between devices with their start and end apart: 12 -> 18, of which waited for: 10 -> 9; matrix products, arithmetic and copies ran while one was open for 14% -> 24% of each run, Pallas kernels for 0% -> 0%
where the time goes in v1:
time: 482 us; the launch traced here: 479 us
  waiting for transfers between devices  215 us (45%)
  blocking collectives  62.3 us (13%)
  local copies, waits for them, and re-layouts  56.1 us (12%)
  other arithmetic  55.9 us (12%)
  loops' own time  28.9 us (6%)
  matrix products  27.1 us (6%)
  between operations  21.7 us (5%)
  starting transfers between devices  12.1 us (3%)
    all_gather x1, waiting for transfers between devices, body(): lax.all_gather(w_conv_in, 'sp', axis=0, tiled=True)  52.9 us
    ppermute x7, waiting for transfers between devices, body(): lax.ppermute(ring[-1], 'sp', [(dev, (dev + 1) % 8) for dev in range(8)])  50.7 us
    all_gather x2, waiting for transfers between devices, carried_in(): pieces = jax.tree.map(lambda part: lax.all_gather(part, axis), value)  40.2 us
    all_gather x2, blocking collectives, carried_in(): pieces = jax.tree.map(lambda part: lax.all_gather(part, axis), value)  35.3 us
    all_gather x1, waiting for transfers between devices, body(): lax.all_gather(w_conv_b, 'sp', axis=0, tiled=True)  32.1 us
    unnamed x78, local copies, waits for them, and re-layouts  29.7 us
    all_gather x1, waiting for transfers between devices, body(): lax.all_gather(w_value, 'sp', axis=0, tiled=True)  29.2 us
    another operation x2, loops' own time, carried_in(): return lax.fori_loop(0, count - 1, lap, subtotal)  28.9 us
  transfers between devices with their start and end apart: 18, of which 9 were waited for; matrix products, arithmetic and copies ran while one was open for 24% of the time, Pallas kernels for 0%

profile of v1, /device:TPU:0, one launch (start us, length us, event | category | flops | bytes accessed | tf_op | source)
XLA Modules:
  0.0 479.5 jit_solution(12625044954124433917)
XLA Ops:
  9.9 3.0 collective-permute-start.2
  28.7 3.7 fusion.90
  39.3 3.6 fusion.93
  44.2 27.0 %all-reduce.8 = (f32[8]{0:T(128)}, f32[8]{0:T(128)}, f32[8]{0:T(128)S(1)}, f32[8]{0:T(128)S(1)}) all-reduce(f32[8]{0:T(128)S(1)} %fusion.71, f32[8]{0:T(128)S(1)} %dynamic-update-slice.1, f32[8]{0:T(128)S(1)} %fusion.70, f32[8]{0:T(128)S(1)} %dynamic-update-slice.3), channel_id=2, replica_groups=mesh['sp'=8,'tp'=4] {'sp'}, use_global_device_ids=true, to_apply=%add.4 | all-reduce | flops 32 | bytes 256
  88.1 20.0 %collective-permute-done.4 = bf16[256,1024]{1,0:T(8,128)(2,1)} collective-permute-done((bf16[256,1024]{1,0:T(8,128)(2,1)}, bf16[256,1024]{1,0:T(8,128)(2,1)}, u32[]{:S(2)}, u32[]{:S(2)}) %collective-permute-start.4) | collective-permute-done | bytes 524320 | tf_op jit(solution)/shard_map/ppermute | solution.py:252
  110.4 14.0 %collective-permute-done.5 = bf16[256,1024]{1,0:T(8,128)(2,1)} collective-permute-done((bf16[256,1024]{1,0:T(8,128)(2,1)}, bf16[256,1024]{1,0:T(8,128)(2,1)}, u32[]{:S(2)}, u32[]{:S(2)}) %collective-permute-start.5) | collective-permute-done | bytes 524320 | tf_op jit(solution)/shard_map/ppermute | solution.py:252
  125.2 2.7 broadcast_multiply_fusion.1
  127.8 16.7 %collective-permute-done.6 = bf16[256,1024]{1,0:T(8,128)(2,1)} collective-permute-done((bf16[256,1024]{1,0:T(8,128)(2,1)}, bf16[256,1024]{1,0:T(8,128)(2,1)}, u32[]{:S(2)}, u32[]{:S(2)}) %collective-permute-start.6) | collective-permute-done | bytes 524320 | tf_op jit(solution)/shard_map/ppermute | solution.py:252
  144.5 29.2 %all-gather.18.cloned.1.call-done = bf16[4096,256]{1,0:T(8,128)(2,1)} async-done(((bf16[512,256]{1,0:T(8,128)(2,1)}), bf16[4096,256]{1,0:T(8,128)(2,1)}) %all-gather.18.cloned.1.call-update) | async-done | bytes 2097168 | tf_op jit(solution)/shard_map/all_gather | solution.py:228
  173.7 2.3 fusion.89
  180.3 17.1 %all_gather.75 = f32[8,1,128]{2,1,0:T(1,128)S(1)} all-gather(f32[1,1,128]{2,1,0:T(1,128)S(1)} %get-tuple-element.431), channel_id=1, replica_groups=mesh['sp'=8,'tp'=4] {'sp'}, dimensions={0}, use_global_device_ids=true | all-gather | bytes 4608 | tf_op jit(solution)/shard_map/all_gather | solution.py:16
  199.4 18.2 %all_gather.69 = f32[8,1,128]{2,1,0:T(1,128)} all-gather(f32[1,1,128]{2,1,0:T(1,128)S(1)} %get-tuple-element.439), channel_id=1, replica_groups=mesh['sp'=8,'tp'=4] {'sp'}, dimensions={0}, use_global_device_ids=true | all-gather | bytes 4608 | tf_op jit(solution)/shard_map/all_gather | solution.py:16
  218.6 6.9 %all-gather.26.cloned.1.call-done = bf16[4096,256]{1,0:T(8,128)(2,1)} async-done(((bf16[512,256]{1,0:T(8,128)(2,1)}), bf16[4096,256]{1,0:T(8,128)(2,1)}) %all-gather.26.cloned.1.call-update) | async-done | bytes 2097168 | tf_op jit(solution)/shard_map/all_gather | solution.py:230
  225.5 2.5 fusion.25
  228.0 52.9 %all-gather.28.cloned.1.call-done = bf16[4096,256]{1,0:T(8,128)(2,1)} async-done(((bf16[512,256]{1,0:T(8,128)(2,1)}), bf16[4096,256]{1,0:T(8,128)(2,1)}) %all-gather.28.cloned.1.call-update) | async-done | bytes 2097168 | tf_op jit(solution)/shard_map/all_gather | solution.py:231
  280.9 2.5 fusion.24
  284.2 3.1 collective-permute-start
  298.5 32.1 %all-gather.24.cloned.1.call-done = bf16[4096,256]{1,0:T(8,128)(2,1)} async-done(((bf16[512,256]{1,0:T(8,128)(2,1)}), bf16[4096,256]{1,0:T(8,128)(2,1)}) %all-gather.24.cloned.1.call-update) | async-done | bytes 2097168 | tf_op jit(solution)/shard_map/all_gather | solution.py:229
  330.6 3.5 fusion.29
  334.1 37.4 %all-gather.20.cloned.1.call-done = f32[8,1,256,128]{3,2,1,0:T(8,128)} async-done(((f32[1,1,256,128]{3,2,1,0:T(8,128)}), f32[8,1,256,128]{3,2,1,0:T(8,128)}) %all-gather.20.cloned.1.call-update) | async-done | bytes 1048592 | tf_op jit(solution)/shard_map/all_gather | solution.py:16
  371.5 38.3 %while.36 = (s32[]{:T(128)}, f32[1,256,128]{2,1,0:T(8,128)S(1)}, f32[1,128]{1,0:T(1,128)}, f32[1]{0:T(128)}, s32[]{:T(128)}, /*index=5*/f32[8,1]{0,1:T(1,128)}, ...) while((s32[]{:T(128)}, f32[1,256,128]{2,1,0:T(8,128)S(1)}, ...), condition=%wide.region_4.5_spmd.clone, body=%wide.region_3.4_spmd.clone.sunk | while | flops 164489 | bytes 395012 | solution.py:28
  409.9 2.8 all-gather.22.cloned.1.call-done
  414.0 23.5 %while.37 = (s32[]{:T(128)}, f32[1,256,128]{2,1,0:T(8,128)S(1)}, f32[1,128]{1,0:T(1,128)S(1)}, f32[1]{0:T(128)}, s32[]{:T(128)}, /*index=5*/f32[8,1]{0,1:T(1,128...) while((s32[]{:T(128)}, f32[1,256,128]{2,1,0:T(8,128)S(1)}, ...), condition=%wide.region_10.11_spmd.clone, body=%wide.region_9.10_spmd.clone.sunk | while | flops 164489 | bytes 395012 | solution.py:28
  468.4 4.6 fusion.15
  (236 shorter events, 123.1 us)
Async XLA Ops:
  6.5 101.6 %all-gather.16.cloned.1.call-start = ((), (), s32[]{:S(2)}) async-start(), calls=%async_computation.1 | async-start | bytes 1179648 | tf_op jit(solution)/shard_map/all_gather | solution.py:227
  7.3 117.9 %all-gather.14.cloned.1.call-start = ((), (), s32[]{:S(2)}) async-start(), calls=%async_computation | async-start | bytes 1179648 | tf_op jit(solution)/shard_map/all_gather | solution.py:226
  8.0 165.7 %all-gather.18.cloned.1.call-start = ((), (), s32[]{:S(2)}) async-start(), calls=%async_computation.2 | async-start | bytes 2359296 | tf_op jit(solution)/shard_map/all_gather | solution.py:228
  8.7 216.7 %all-gather.26.cloned.1.call-start = ((), (), s32[]{:S(2)}) async-start(), calls=%async_computation.6 | async-start | bytes 2359296 | tf_op jit(solution)/shard_map/all_gather | solution.py:230
  9.3 271.6 %all-gather.28.cloned.1.call-start = ((), (), s32[]{:S(2)}) async-start(), calls=%async_computation.7 | async-start | bytes 2359296 | tf_op jit(solution)/shard_map/all_gather | solution.py:231
  9.9 320.7 %all-gather.24.cloned.1.call-start = ((), (), s32[]{:S(2)}) async-start(), calls=%async_computation.5 | async-start | bytes 2359296 | tf_op jit(solution)/shard_map/all_gather | solution.py:229
  9.9 27.0 %collective-permute-start.2 = (bf16[256,1024]{1,0:T(8,128)(2,1)}, bf16[256,1024]{1,0:T(8,128)(2,1)S(1)}, u32[]{:S(2)}, u32[]{:S(2)}) collective-permute-start(bf16[256,1024]{1,0:T(8,128)(2,1)} %param.33), channel_id=1, source_target_pairs={{0,4},{4,8},{8,12},{12,16},{16,20},{20,24},{24,28},{28,0},{1,5},{5... | collective-permute-start | bytes 1572872 | tf_op jit(solution)/shard_map/ppermute | solution.py:252
  13.0 358.5 %all-gather.20.cloned.1.call-start = ((), (), s32[]{:S(2)}) async-start(), calls=%async_computation.3 | async-start | bytes 1179648 | tf_op jit(solution)/shard_map/all_gather | solution.py:16
  37.0 47.3 %collective-permute-start.3 = (bf16[256,1024]{1,0:T(8,128)(2,1)S(1)}, bf16[256,1024]{1,0:T(8,128)(2,1)}, u32[]{:S(2)}, u32[]{:S(2)}) collective-permute-start(bf16[256,1024]{1,0:T(8,128)(2,1)S(1)} %collective-permute-done.2), channel_id=1, source_target_pairs={{0,4},{4,8},{8,12},{12,16},{16,20},{20,24},{24,28},{28,0},{1,5},{5... | collective-permute-start | bytes 1572872 | tf_op jit(solution)/shard_map/ppermute | solution.py:252
  84.3 23.8 %collective-permute-start.4 = (bf16[256,1024]{1,0:T(8,128)(2,1)}, bf16[256,1024]{1,0:T(8,128)(2,1)}, u32[]{:S(2)}, u32[]{:S(2)}) collective-permute-start(bf16[256,1024]{1,0:T(8,128)(2,1)} %collective-permute-done.3), channel_id=1, source_target_pairs={{0,4},{4,8},{8,12},{12,16},{16,20},{20,24},{24,28},{28,0},{1,5},{5... | collective-permute-start | bytes 1572872 | tf_op jit(solution)/shard_map/ppermute | solution.py:252
  108.1 16.3 %collective-permute-start.5 = (bf16[256,1024]{1,0:T(8,128)(2,1)}, bf16[256,1024]{1,0:T(8,128)(2,1)}, u32[]{:S(2)}, u32[]{:S(2)}) collective-permute-start(bf16[256,1024]{1,0:T(8,128)(2,1)} %collective-permute-done.4), channel_id=1, source_target_pairs={{0,4},{4,8},{8,12},{12,16},{16,20},{20,24},{24,28},{28,0},{1,5},{5... | collective-permute-start | bytes 1572872 | tf_op jit(solution)/shard_map/ppermute | solution.py:252
  124.4 20.1 %collective-permute-start.6 = (bf16[256,1024]{1,0:T(8,128)(2,1)}, bf16[256,1024]{1,0:T(8,128)(2,1)}, u32[]{:S(2)}, u32[]{:S(2)}) collective-permute-start(bf16[256,1024]{1,0:T(8,128)(2,1)} %collective-permute-done.5), channel_id=1, source_target_pairs={{0,4},{4,8},{8,12},{12,16},{16,20},{20,24},{24,28},{28,0},{1,5},{5... | collective-permute-start | bytes 1572872 | tf_op jit(solution)/shard_map/ppermute | solution.py:252
  144.5 73.7 %collective-permute-start.7 = (bf16[256,1024]{1,0:T(8,128)(2,1)}, bf16[256,1024]{1,0:T(8,128)(2,1)}, u32[]{:S(2)}, u32[]{:S(2)}) collective-permute-start(bf16[256,1024]{1,0:T(8,128)(2,1)} %collective-permute-done.6), channel_id=1, source_target_pairs={{0,4},{4,8},{8,12},{12,16},{16,20},{20,24},{24,28},{28,0},{1,5},{5... | collective-permute-start | bytes 1572872 | tf_op jit(solution)/shard_map/ppermute | solution.py:252
  178.8 233.9 %all-gather.22.cloned.1.call-start = ((), (), s32[]{:S(2)}) async-start(), calls=%async_computation.4 | async-start | bytes 1179648 | tf_op jit(solution)/shard_map/all_gather | solution.py:16
  218.2 72.8 %collective-permute-start.8 = (bf16[256,1024]{1,0:T(8,128)(2,1)}, bf16[256,1024]{1,0:T(8,128)(2,1)}, u32[]{:S(2)}, u32[]{:S(2)}) collective-permute-start(bf16[256,1024]{1,0:T(8,128)(2,1)} %collective-permute-done.7), channel_id=1, source_target_pairs={{0,4},{4,8},{8,12},{12,16},{16,20},{20,24},{24,28},{28,0},{1,5},{5... | collective-permute-start | bytes 1572872 | tf_op jit(solution)/shard_map/ppermute | solution.py:252
  284.2 12.5 %collective-permute-start = (bf16[1,256]{0,1:T(8,128)(2,1)}, bf16[1,256]{0,1:T(8,128)(2,1)}, u32[]{:S(2)}, u32[]{:S(2)}) collective-permute-start(bf16[1,256]{0,1:T(8,128)(2,1)} %get-tuple-element.447), channel_id=1, source_target_pairs={{0,4},{4,8},{8,12},{12,16},{16,20},{20,24},{24,28},{1,5},{5,9},{9,... | collective-permute-start | bytes 1544 | tf_op jit(solution)/shard_map/ppermute | solution.py:38
  287.3 9.4 %collective-permute-start.1 = (bf16[1,256]{0,1:T(8,128)(2,1)}, bf16[1,256]{0,1:T(8,128)(2,1)}, u32[]{:S(2)}, u32[]{:S(2)}) collective-permute-start(bf16[1,256]{0,1:T(8,128)(2,1)} %get-tuple-element.448), channel_id=1, source_target_pairs={{4,0},{8,4},{12,8},{16,12},{20,16},{24,20},{28,24},{5,1},{9,5},{13... | collective-permute-start | bytes 1544 | tf_op jit(solution)/shard_map/ppermute | solution.py:39
  290.8 177.6 %all-gather.30.cloned.1.call-start = ((), (), s32[]{:S(2)}) async-start(), calls=%async_computation.8 | async-start | bytes 1310720 | tf_op jit(solution)/shard_map/all_gather | solution.py:249
  334.1 107.8 %copy-start.9 = (f32[1,2,128]{2,1,0:T(2,128)S(1)}, f32[1,2,128]{2,1,0:T(2,128)}, u32[]{:S(2)}) copy-start(f32[1,2,128]{2,1,0:T(2,128)} %copy-done.8) | copy-start | bytes 3076
  334.1 107.8 %copy-start.11 = (f32[1,2,128]{2,1,0:T(2,128)S(1)}, f32[1,2,128]{2,1,0:T(2,128)}, u32[]{:S(2)}) copy-start(f32[1,2,128]{2,1,0:T(2,128)} %copy-done.10) | copy-start | bytes 3076
  334.1 107.8 %copy-start.22 = (f32[2,128]{1,0:T(2,128)S(1)}, f32[2,128]{1,0:T(2,128)}, u32[]{:S(2)}) copy-start(f32[2,128]{1,0:T(2,128)} %get-tuple-element.383) | copy-start | bytes 3076
  334.1 107.8 %copy-start.23 = (f32[2,128]{1,0:T(2,128)S(1)}, f32[2,128]{1,0:T(2,128)}, u32[]{:S(2)}) copy-start(f32[2,128]{1,0:T(2,128)} %get-tuple-element.384) | copy-start | bytes 3076
  334.1 107.9 %copy-start.13 = (f32[1,256]{1,0:T(1,128)S(1)}, f32[1,256]{1,0:T(1,128)}, u32[]{:S(2)}) copy-start(f32[1,256]{1,0:T(1,128)} %copy-done.12) | copy-start | bytes 3076
  334.1 108.8 %copy-start.7 = (f32[1,1,256,128]{3,2,1,0:T(8,128)S(1)}, f32[1,1,256,128]{3,2,1,0:T(8,128)}, u32[]{:S(2)}) copy-start(f32[1,1,256,128]{3,2,1,0:T(8,128)} %get-tuple-element.434) | copy-start | bytes 393220
  (22 other events, 1231.4 us)
Sparse Core Ops, SparseCore 0:
  9.5 50.9 all-gather.15
  62.6 43.5 all-gather.13
  108.3 65.3 all-gather.17
  175.7 49.7 all-gather.25
  227.5 53.4 all-gather.27
  282.9 47.6 all-gather.23
  332.7 38.7 all-gather.19
  373.7 38.9 all-gather.21
  448.1 15.4 all-gather.29
